TPU v7x, 32 devices: a whole 2x2x4 slice. The times are simulated.
32 devices in a mesh: grp: 2 (over y), sp: 4 (over z), fs: 2 (over x), tp: 2 (over core).
Axes of the slice: x: 2, y: 2, z: 4, core: 2. Of those that a mesh axis runs over, the one named last changes fastest.
Arguments:
- tokens: bfloat16 [8, 256, 2048], P(('grp', 'fs'), 'sp'), parts along dimension 0, may hold values from -6 to 6
- pre_gain: float32 [2048], replicated, may hold values from 0.1 to 1.9
- query_weight: bfloat16 [2048, 1024], P(('sp', 'fs'), 'tp'), may hold values from -0.125 to 0.125
- key_weight: bfloat16 [2048, 1024], P(('sp', 'fs'), 'tp'), may hold values from -0.125 to 0.125
- value_weight: bfloat16 [2048, 1024], P(('sp', 'fs'), 'tp'), may hold values from -0.125 to 0.125
- beta_weight: bfloat16 [2048, 8], replicated, may hold values from -0.125 to 0.125
- decay_weight: bfloat16 [2048, 8], replicated, may hold values from -0.125 to 0.125
- decay_rate: float32 [8], replicated, may hold values from 0 to 1
- delta_gain: float32 [128], replicated, may hold values from 0.1 to 1.9
- query_down: bfloat16 [2048, 512], P(('sp', 'fs')), may hold values from -0.125 to 0.125
- latent_down: bfloat16 [2048, 256], P(('sp', 'fs')), may hold values from -0.125 to 0.125
- rope_weight: bfloat16 [2048, 32], replicated, may hold values from -0.125 to 0.125
- query_gain: float32 [512], replicated, may hold values from 0.1 to 1.9
- latent_gain: float32 [256], replicated, may hold values from 0.1 to 1.9
- query_up: bfloat16 [512, 1536], P(None, 'tp'), may hold values from -4 to 4
- latent_up: bfloat16 [256, 2048], P(None, 'tp'), may hold values from -4 to 4
- delta_out: bfloat16 [1024, 2048], P('tp', ('sp', 'fs')), may hold values from -8 to 8
- latent_out: bfloat16 [1024, 2048], P('tp', ('sp', 'fs')), may hold values from -8 to 8
- post_gain: float32 [2048], P('tp'), may hold values from 0.1 to 1.9
Outputs:
- mixed_out: bfloat16 [8, 256, 2048], P(('grp', 'fs'), 'sp', 'tp'), parts along dimension 0
There are 2 independent parts, one for each index of `grp`. A program takes and returns all parts, laid end to end along the dimension named above; an argument that names none is the same for every part. Nothing has to cross between parts.
All inputs are finite; a program needn't handle non-finite values.
Results may differ from a plain program's by a relative error of at most 0.018.
The roundings to bfloat16 on the way count: a program that leaves them out, or rounds other values in their place, can miss the bound.
Values may be sent and summed in bfloat16 or wider, within the bound.
A program may use at most 128 MiB of HBM per device.

v0:
```python
import functools
import math

import jax
import jax.numpy as jnp
from jax import lax
from jax.experimental import pallas as pl
from jax.experimental.pallas import tpu as pltpu
from jax.sharding import PartitionSpec as P

HEAD = 128
NOPE = 64
ROPE = 32
VDIM = 64
BLOCK = 64
NORM_EPS = 1e-06
ROPE_THETA = 10000.0
HIGHEST = lax.Precision.HIGHEST
MESH = pl.DeviceIdType.MESH
F32 = jnp.float32
BF16 = jnp.bfloat16


def dot(a, b, precision=None):
    return jnp.dot(a, b, preferred_element_type=F32, precision=precision)


def dot_t(a, b, precision=None):
    return lax.dot_general(
        a, b, (((1,), (1,)), ((), ())), preferred_element_type=F32, precision=precision
    )


def t_dot(a, b, precision=None):
    return lax.dot_general(
        a, b, (((0,), (0,)), ((), ())), preferred_element_type=F32, precision=precision
    )


def when(cond, fn):
    if cond is True:
        fn()
    elif cond is not False:
        pl.when(cond)(fn)


def both(a, b):
    if a is True:
        return b
    if b is True:
        return a
    return jnp.logical_and(a, b)


class Place:
    def __init__(self, sizes):
        self.Y, self.Z, self.X, self.C = sizes
        self.y = lax.axis_index("grp")
        self.z = lax.axis_index("sp")
        self.x = lax.axis_index("fs")
        self.c = lax.axis_index("tp")


def greet(place, plane=True, later=False):
    barrier = pltpu.get_barrier_semaphore()

    def signal(cond, dev):
        when(
            cond,
            lambda: pl.semaphore_signal(barrier, inc=1, device_id=dev, device_id_type=MESH),
        )

    count = jnp.int32(0)
    if later:
        for k in range(1, place.Z):
            signal(place.z + k < place.Z, {"sp": place.z + k})
            signal(place.z - k >= 0, {"sp": place.z - k})
        count += place.Z - 1
    else:
        signal(place.z + 1 < place.Z, {"sp": place.z + 1})
        signal(place.z > 0, {"sp": place.z - 1})
        count += (place.z + 1 < place.Z).astype(jnp.int32) + (place.z > 0).astype(jnp.int32)
    if plane:
        for d in range(1, place.X):
            signal(True, {"fs": lax.rem(place.x + d, place.X)})
        count += place.X - 1
        if place.Y == 2:
            signal(True, {"grp": 1 - place.y})
            count += 1
    signal(True, {"tp": 1 - place.c})
    count += 1
    pl.semaphore_wait(barrier, count)


class Gather:
    def __init__(self, place, own, buf, send, recv, lsem):
        self.pl, self.own, self.buf = place, own, buf
        self.send, self.recv, self.lsem = send, recv, lsem
        self.sends = []
        self.ev = 0

    def active(self, p):
        return True if p == 2 else self.pl.y == p

    def push(self, cond, src, p, slot, dev, ev, way):
        index = len(self.sends)

        def make():
            return pltpu.make_async_remote_copy(
                src_ref=src,
                dst_ref=self.buf(p, slot),
                send_sem=self.send.at[index],
                recv_sem=self.recv.at[slot, p],
                device_id=dev,
                device_id_type=MESH,
            )

        when(cond, lambda: make().start())
        self.sends.append((cond, make))

    def arrived(self, cond, p, slot):
        def wait():
            ref = self.buf(p, slot)
            pltpu.make_async_remote_copy(
                src_ref=ref,
                dst_ref=ref,
                send_sem=self.lsem.at[p],
                recv_sem=self.recv.at[slot, p],
                device_id={"tp": self.pl.c},
                device_id_type=MESH,
            ).wait_recv()

        when(cond, wait)

    def across(self, cond, src, p, slot, ev):
        q = self.pl
        for d in range(1, q.X):
            self.push(cond, src, p, slot, {"fs": lax.rem(q.x + d, q.X)}, ev, 1 + d)

    def to_y(self, cond, src, p, slot, ev):
        if p < 2:
            self.push(cond, src, p, slot, {"grp": 1 - self.pl.y}, ev, 0)

    def kinds(self):
        return (0, 1, 2)

    def start_along(self):
        q = self.pl
        me = q.z * q.X + q.x
        for p in self.kinds():
            a = self.active(p)
            src = self.own(p)
            self.push(both(a, q.z + 1 < q.Z), src, p, me, {"sp": q.z + 1}, 0, 0)
            self.push(both(a, q.z > 0), src, p, me, {"sp": q.z - 1}, 0, 1)

    def start_across(self):
        q = self.pl
        me = q.z * q.X + q.x
        for p in self.kinds():
            self.across(self.active(p), self.own(p), p, me, 0)
        for p in self.kinds():
            pltpu.make_async_copy(self.own(p), self.buf(p, me), self.lsem.at[p]).start()

    def step(self, k):
        q = self.pl
        for p in self.kinds():
            a = self.active(p)
            for sign in (1, -1):
                zz = q.z - sign * k
                ok = both(a, jnp.logical_and(zz >= 0, zz < q.Z))
                slot = zz * q.X + q.x
                nxt = q.z + sign
                ev = 2 * k - (sign == 1)
                self.arrived(ok, p, slot)
                ref = self.buf(p, slot)
                self.push(
                    both(ok, jnp.logical_and(nxt >= 0, nxt < q.Z)),
                    ref, p, slot, {"sp": nxt}, ev, 1,
                )
                self.across(ok, ref, p, slot, ev)
                self.to_y(ok, ref, p, slot, ev)

    def cross_step(self, k):
        q = self.pl
        base = 2 * q.Z
        for p in self.kinds():
            a = self.active(p)
            for sign in (1, -1) if k else (1,):
                zz = q.z - sign * k
                ok = both(a, jnp.logical_and(zz >= 0, zz < q.Z))
                for d in range(1, q.X):
                    slot = zz * q.X + lax.rem(q.x + d, q.X)
                    ev = base + (2 * k - (sign == 1) + 1) * (q.X - 1) + d - 1
                    self.arrived(ok, p, slot)
                    self.to_y(ok, self.buf(p, slot), p, slot, ev)

    def finish(self):
        q = self.pl
        self.cross_step(q.Z - 1)
        me = q.z * q.X + q.x
        for p in (0, 1):
            for s in range(q.Z * q.X):
                self.arrived(jnp.logical_and(q.y != p, me != s), p, s)
        for p in self.kinds():
            pltpu.make_async_copy(self.own(p), self.buf(p, me), self.lsem.at[p]).wait()

    def drain(self):
        for cond, make in self.sends:
            when(cond, lambda make=make: make().wait_send())

    @staticmethod
    def scratch(Z, X):
        n = Z * X
        sends = 3 * (X + 1) + 2 * (Z - 1) * (3 * X + 2) + (2 * Z - 1) * (X - 1) * 2
        return [
            pltpu.SemaphoreType.DMA((sends,)),
            pltpu.SemaphoreType.DMA((n, 3)),
            pltpu.SemaphoreType.DMA((3,)),
        ]


def spread(copies, parts, target, bounds):
    at = 0
    for ref, offset, width in parts:
        done = 0
        while done < width:
            p, col = divmod(at + done, bounds)
            size = min(width - done, bounds - col)
            start = offset + done
            if not isinstance(start, int):
                start = pl.multiple_of(start, 128)
            copies.append((ref.at[:, pl.ds(start, size)], target.at[p, :, pl.ds(col, size)]))
            done += size
        at += width


def back_kernel(
    sizes, seqs, heads, cuts, tokens, pre_gain, small, w_query, w_key, w_value, w_qdown, w_kdown,
    w_delta, w_latent, qgain, kgain, w_qup, w_lup, rate_in, gain, post,
    out, qup, lup, raw, lat, rate, own1, own, buf1, kvr, kbuf, sin, sout, hbuf, buf, pbuf, rbuf, sq,
    asem, ksem, ssem, send1, recv1, lsem1, send, recv, lsem, tsem,
):
    place = Place(sizes)
    Z, z, c = place.Z, place.z, place.c
    C = sizes[3]
    rows = tokens.shape[0]
    third = own1.shape[2]
    qcols, kcols = w_qdown.shape[1] // C, w_kdown.shape[1] // C
    pairs = []
    spread(
        pairs,
        [(w, 0, w.shape[1]) for w in (w_query, w_key, w_value)]
        + [(w_qdown, c * qcols, qcols), (w_kdown, c * kcols, kcols)],
        own1, third,
    )
    upper = w_delta.shape[0]
    pairs.append((w_delta, own.at[pl.ds(0, upper)]))
    pairs.append((w_latent, own.at[pl.ds(upper, w_latent.shape[0])]))
    loads = [pltpu.make_async_copy(a, b, asem.at[i]) for i, (a, b) in enumerate(pairs)]
    for load in loads:
        load.start()
    greet(place, later=True)
    for load in loads:
        load.wait()
    g1 = Gather(
        place, lambda p: own1.at[p], lambda p, s: buf1.at[p, s], send1, recv1, lsem1
    )
    g = Gather(
        place,
        lambda p: own.at[pl.ds(cuts[p], cuts[p + 1] - cuts[p])],
        lambda p, s: buf.at[s, pl.ds(cuts[p], cuts[p + 1] - cuts[p])],
        send, recv, lsem,
    )
    g1.start_along()
    g1.start_across()
    x = tokens[...].astype(F32)
    xscale = lax.rsqrt(jnp.mean(x * x, axis=-1, keepdims=True) + NORM_EPS)
    normed = (x * xscale * pre_gain[...]).astype(BF16)
    sm_all = dot_t(normed, small[...])
    qcol = w_qup.shape[1]
    lh = qcol // (NOPE + ROPE)
    turn_w = ROPE // 2
    kinds = ((NOPE, 0, qup, w_qup, NOPE + ROPE), (turn_w, NOPE, qup, w_qup, NOPE + ROPE),
             (turn_w, NOPE + turn_w, qup, w_qup, NOPE + ROPE),
             (NOPE, 0, lup, w_lup, NOPE + VDIM), (VDIM, NOPE, lup, w_lup, NOPE + VDIM))
    fill_at = {}
    for w, off, to, frm, per in kinds:
        size = lh * w
        dst_i = lax.broadcasted_iota(jnp.int32, (frm.shape[1], size), 1)
        src_i = lax.broadcasted_iota(jnp.int32, (frm.shape[1], size), 0)
        perm = jnp.where(src_i == dst_i // w * per + off + dst_i % w, 1.0, 0.0).astype(BF16)
        lo = fill_at.get(per, 0)
        to[:, lo : lo + size] = dot(frm[...], perm).astype(BF16)
        fill_at[per] = lo + size
    for k in range(1, Z):
        g1.step(k)
        g1.cross_step(k - 1)
        if k == max(1, Z - 2):
            g.start_along()
    g.start_across()
    if Z > 1:
        g.step(1)
    g1.finish()
    depth1 = buf1.shape[1] * buf1.shape[2]
    part2 = dot(normed, buf1[2].reshape(depth1, third)).astype(BF16)
    lat[c] = part2[:, third - qcols - kcols :]
    trade = pltpu.make_async_remote_copy(
        src_ref=lat.at[c], dst_ref=lat.at[c], send_sem=tsem.at[4], recv_sem=tsem.at[5],
        device_id={"tp": 1 - c}, device_id_type=MESH,
    )
    trade.start()
    raw[:, 2 * third : 3 * third] = part2
    for p in range(2):
        raw[:, p * third : (p + 1) * third] = dot(
            normed, buf1[p].reshape(depth1, third)
        ).astype(BF16)
    trade.wait()
    qw = qup.shape[0] // sizes[3]
    kw_lat = lup.shape[0] // sizes[3]
    tile = 128
    lane = lax.broadcasted_iota(jnp.int32, (rows, tile), 1)
    half_turn = ROPE // 2
    step = (lane % half_turn).astype(F32)
    row = lax.broadcasted_iota(jnp.int32, (rows, tile), 0)
    pos = (z * BLOCK + row % BLOCK).astype(F32)
    angle = pos * jnp.exp(step * (-2.0 * math.log(ROPE_THETA) / ROPE))
    cos, sin_t = jnp.cos(angle), jnp.sin(angle)

    def normed_parts(lo, w, g):
        parts = [lat[i, :, lo : lo + w].astype(F32) for i in range(sizes[3])]
        squares = sum(jnp.sum(p * p, axis=-1, keepdims=True) for p in parts)
        scale = lax.rsqrt(squares / (w * sizes[3]) + NORM_EPS)
        return [
            (p * scale * g[:, i * w : (i + 1) * w]).astype(BF16) for i, p in enumerate(parts)
        ]

    kparts = normed_parts(qw, kw_lat, kgain)
    krank = kw_lat * sizes[3]
    for i, p in enumerate(kparts):
        kvr[:, i * kw_lat : (i + 1) * kw_lat] = p
    allheads = heads * C
    src = lax.broadcasted_iota(jnp.int32, (tile, tile), 0)
    dst = lax.broadcasted_iota(jnp.int32, (tile, tile), 1)
    rope_raw = sm_all.astype(BF16)
    base = 2 * allheads + dst % half_turn

    def pick(cond, kind):
        return jnp.where(cond, 1.0, 0.0).astype(kind)

    rlo = dot(rope_raw, pick(src == base, BF16))
    rhi = dot(rope_raw, pick(src == base + half_turn, BF16))
    left = lane < tile // 2
    kvr[:, krank : krank + tile] = jnp.where(
        left, rlo * cos - rhi * sin_t, rhi * cos + rlo * sin_t
    ).astype(BF16)

    def kv_copy(k):
        return pltpu.make_async_remote_copy(
            src_ref=kvr,
            dst_ref=kbuf.at[z],
            send_sem=ksem.at[0, k],
            recv_sem=ksem.at[1, z],
            device_id={"sp": z + k},
            device_id_type=MESH,
        )

    for k in range(1, Z):
        when(z + k < Z, lambda k=k: kv_copy(k).start())
    ri = lax.broadcasted_iota(jnp.int32, (rows, rows), 0)
    ci = lax.broadcasted_iota(jnp.int32, (rows, rows), 1)
    tri = jnp.where((ri >= ci) & (ri // BLOCK == ci // BLOCK), 1.0, 0.0).astype(F32)
    rate[...] = jnp.zeros(rate.shape, F32)
    rate[:, allheads : 2 * allheads] = rate_in[...]
    first_head = c * heads
    own_beta = pick((dst < heads) & (src == first_head + dst), F32)
    own_rate = pick(
        (dst >= heads) & (dst < 2 * heads) & (src == allheads + first_head + dst - heads), F32
    )
    pre = dot(sm_all, own_beta + own_rate, HIGHEST)
    rates = dot(jnp.broadcast_to(rate[...], (8, tile)), own_rate, HIGHEST)[:1]
    beta_all = jax.nn.sigmoid(pre)
    log_a = -rates * (jnp.maximum(pre, 0.0) + jnp.log1p(jnp.exp(-jnp.abs(pre))))
    gates = dot(tri, log_a, HIGHEST)
    gates_t = gates.T
    r = lax.broadcasted_iota(jnp.int32, (BLOCK, BLOCK), 0)
    cc = lax.broadcasted_iota(jnp.int32, (BLOCK, BLOCK), 1)
    strict = r > cc
    causal = r >= cc
    eye = jnp.where(r == cc, 1.0, 0.0).astype(F32)
    lanes = [(b, h) for b in range(seqs) for h in range(heads)]
    width = heads * HEAD
    terms = []
    for b, h in lanes:
        t = slice(b * BLOCK, (b + 1) * BLOCK)

        def act(i):
            v = raw[t, i * width + h * HEAD : i * width + (h + 1) * HEAD].astype(F32)
            return v * jax.nn.sigmoid(v)

        def unit(u):
            return u * lax.rsqrt(jnp.sum(u * u, axis=-1, keepdims=True) + NORM_EPS)

        q = unit(act(0)) * HEAD ** (-0.5)
        k = unit(act(1))
        v = act(2)
        beta = beta_all[t, h : h + 1]
        gcol = gates[t, heads + h : heads + h + 1]
        grow = gates_t[heads + h : heads + h + 1, t]
        glast = gates[(b + 1) * BLOCK - 1 : (b + 1) * BLOCK, heads + h : heads + h + 1]
        gap = gcol - grow
        decay = jnp.where(causal, jnp.exp(jnp.where(causal, gap, 0.0)), 0.0)
        ks = k * beta
        low = jnp.where(strict, dot_t(ks, k, HIGHEST) * decay, 0.0)
        scores = dot_t(q.astype(BF16), k.astype(BF16)) * decay
        eg = jnp.exp(gcol)
        terms.append([low, scores, v * beta, ks * eg, q * eg, k * jnp.exp(glast - gcol),
                      jnp.exp(glast)])
    every = range(len(lanes))
    inv = [eye - jnp.where((r // 2 == cc // 2), terms[i][0], 0.0) for i in every]
    size = 2
    while size < BLOCK:
        joint = (r // (2 * size) == cc // (2 * size)) & (r // size != cc // size)
        mids = [dot(jnp.where(joint, terms[i][0], 0.0), inv[i], HIGHEST) for i in every]
        inv = [inv[i] - dot(inv[i], mids[i], HIGHEST) for i in every]
        size *= 2
    inv = [m.astype(BF16) for m in inv]
    nv = [dot(inv[i], terms[i][2].astype(BF16)) for i in every]
    kw = [dot(inv[i], terms[i][3].astype(BF16)) for i in every]

    def state_copy(i):
        return pltpu.make_async_remote_copy(
            src_ref=sout.at[i],
            dst_ref=sin.at[i],
            send_sem=ssem.at[0, i],
            recv_sem=ssem.at[1, i],
            device_id={"sp": z + 1},
            device_id_type=MESH,
        )

    g.cross_step(0)
    if Z > 2:
        g.step(2)
    for i, (b, h) in enumerate(lanes):
        low, scores, vb, ke, qd, kd, factor = terms[i]

        def clear(i=i):
            sin[i] = jnp.zeros((HEAD, HEAD), BF16)

        when(z == 0, clear)
        when(z > 0, lambda i=i: state_copy(i).wait_recv())
        s_in = sin[i]
        corrected = nv[i] - dot(kw[i].astype(BF16), s_in)
        sout[i] = (
            s_in.astype(F32) * factor + t_dot(kd.astype(BF16), corrected.astype(BF16))
        ).astype(BF16)
        when(z + 1 < Z, lambda i=i: state_copy(i).start())
        o = dot(qd.astype(BF16), s_in) + dot(scores.astype(BF16), corrected.astype(BF16))
        o = o * lax.rsqrt(jnp.mean(o * o, axis=-1, keepdims=True) + NORM_EPS) * gain[...]
        hbuf[b * BLOCK : (b + 1) * BLOCK, h * HEAD : (h + 1) * HEAD] = o.astype(BF16)
    g.cross_step(1)
    for k in range(3, Z):
        g.step(k)
        if k < Z - 1:
            g.cross_step(k - 1)

    for k in range(1, Z):
        def take(k=k):
            pltpu.make_async_remote_copy(
                src_ref=kvr, dst_ref=kbuf.at[z - k], send_sem=ksem.at[0, k],
                recv_sem=ksem.at[1, z - k], device_id={"sp": z}, device_id_type=MESH,
            ).wait_recv()

        when(z - k >= 0, take)
    for s in range(Z):
        def fill(s=s):
            kbuf[s] = kvr[...]

        def none(s=s):
            kbuf[s] = jnp.zeros(kbuf.shape[1:], BF16)

        when(z == s, fill)
        when(z < s, none)
    qparts = normed_parts(0, qw, qgain)
    qa = sum(dot(p, qup[i * qw : (i + 1) * qw, :]) for i, p in enumerate(qparts)).astype(BF16)
    plain_width = qa.shape[1] - 2 * tile
    qlo_raw = qa[:, plain_width : plain_width + tile].astype(F32)
    qhi_raw = qa[:, plain_width + tile :].astype(F32)
    qlo = (qlo_raw * cos - qhi_raw * sin_t).astype(BF16)
    qhi = (qhi_raw * cos + qlo_raw * sin_t).astype(BF16)
    lane1 = lax.broadcasted_iota(jnp.int32, (1, tile), 1)

    def keep(cond):
        return jnp.where(cond, 1.0, 0.0).astype(BF16)

    keys = Z * BLOCK
    allowed = lax.broadcasted_iota(jnp.int32, (2 * BLOCK, keys), 1) // BLOCK <= z
    left_half = lax.broadcasted_iota(jnp.int32, (BLOCK, tile), 1) < tile // 2
    for b in range(seqs):
        t = slice(b * BLOCK, (b + 1) * BLOCK)
        kv = jnp.concatenate([kbuf[s, t, :] for s in range(Z)], axis=0)
        up = dot(kv[:, :krank], lup[...]).astype(BF16)
        turn = kv[:, krank : krank + tile].astype(F32)
        rolled = pltpu.roll(turn, tile // 2, 1)
        sel = lax.broadcasted_iota(jnp.int32, (keys, tile), 1) < tile // 2
        klo = jnp.where(sel, turn, rolled).astype(BF16)
        khi = jnp.where(sel, rolled, turn).astype(BF16)
        for j in range(plain_width // tile):
            at = slice(j * tile, (j + 1) * tile)
            qp = qa[t, at]
            first, second = keep(lane1 < tile // 2), keep(lane1 >= tile // 2)
            m0, m1 = keep(lane1 // half_turn == 2 * j), keep(lane1 // half_turn == 2 * j + 1)
            s = (
                dot_t(jnp.concatenate([qp * first, qp * second], axis=0), up[:, at])
                + dot_t(jnp.concatenate([qlo[t] * m0, qlo[t] * m1], axis=0), klo)
                + dot_t(jnp.concatenate([qhi[t] * m0, qhi[t] * m1], axis=0), khi)
            ) * (NOPE + ROPE) ** (-0.5)
            s = jnp.where(allowed, s, -jnp.inf)
            w = jnp.exp(s - jnp.max(s, axis=-1, keepdims=True))
            o = dot(w.astype(BF16), up[:, plain_width + j * tile : plain_width + (j + 1) * tile])
            o = o / jnp.sum(w, axis=-1, keepdims=True)
            hbuf[t, width + j * tile : width + (j + 1) * tile] = jnp.where(
                left_half, o[:BLOCK], o[BLOCK:]
            ).astype(BF16)
    if Z > 3:
        g.cross_step(Z - 2)
    g.finish()
    n = buf.shape[0]
    half = n // 2
    hv = hbuf[...]

    def part(s, carry):
        pbuf[s] = dot(hv, buf[s]).astype(BF16)
        return carry

    lax.fori_loop(0, n, part, 0)
    peer = 1 - c
    copy = pltpu.make_async_remote_copy(
        src_ref=pbuf.at[pl.ds(peer * half, half)],
        dst_ref=rbuf,
        send_sem=tsem.at[0],
        recv_sem=tsem.at[1],
        device_id={"tp": peer},
        device_id_type=MESH,
    )
    copy.start()
    g1.drain()
    g.drain()
    for k in range(1, Z):
        when(z + k < Z, lambda k=k: kv_copy(k).wait_send())
    for i in every:
        when(z + 1 < Z, lambda i=i: state_copy(i).wait_send())
    copy.wait()
    total = jnp.zeros((rows, 1), F32)
    mixed = []
    for s in range(half):
        m = pbuf[c * half + s].astype(F32) + rbuf[s].astype(F32)
        mixed.append(m)
        total = total + jnp.sum(m * m, axis=-1, keepdims=True)
    sq[0] = jnp.broadcast_to(total, sq.shape[1:])
    squares = pltpu.make_async_remote_copy(
        src_ref=sq.at[0],
        dst_ref=sq.at[1],
        send_sem=tsem.at[2],
        recv_sem=tsem.at[3],
        device_id={"tp": peer},
        device_id_type=MESH,
    )
    squares.start()
    squares.wait()
    total = total + sq[1][:, :1]
    cb = buf.shape[2]
    scale = lax.rsqrt(total / (n * cb) + NORM_EPS)
    for s in range(half):
        out[:, s * cb : (s + 1) * cb] = (mixed[s] * scale * post[s]).astype(BF16)


def vmem():
    return pl.BlockSpec(memory_space=pltpu.VMEM)


def anywhere():
    return pl.BlockSpec(memory_space=pl.ANY)


def local(
    sizes,
    tokens, pre_gain, query_weight, key_weight, value_weight, beta_weight, decay_weight,
    decay_rate, delta_gain, query_down, latent_down, rope_weight, query_gain, latent_gain,
    query_up, latent_up, delta_out, latent_out, post_gain,
):
    Y, Z, X, C = sizes
    n = Z * X
    seqs, count, width = tokens.shape
    rows = seqs * count
    qw = query_down.shape[1] // C
    kw = latent_down.shape[1] // C
    heads = query_weight.shape[1] // HEAD
    shard = query_weight.shape[0]
    third = (3 * query_weight.shape[1] + qw + kw) // 3
    small = [beta_weight.T, decay_weight.T, rope_weight.T]
    used = sum(w.shape[0] for w in small)
    small = jnp.concatenate(small + [jnp.zeros((128 - used, width), BF16)], axis=0)
    lanes = seqs * heads
    cb = delta_out.shape[1]
    depth = delta_out.shape[0] + latent_out.shape[0]
    cuts = (0, depth * 3 // 8, depth * 6 // 8, depth)
    half = n // 2
    kv_width = latent_down.shape[1] + 128
    args = (
        tokens.reshape(rows, width), pre_gain.reshape(1, width), small,
        query_weight, key_weight, value_weight, query_down, latent_down, delta_out, latent_out,
        query_gain.reshape(1, -1), latent_gain.reshape(1, -1), query_up, latent_up,
        decay_rate.reshape(1, -1), delta_gain.reshape(1, HEAD), post_gain.reshape(half, 1, cb),
    )
    result = pl.pallas_call(
        functools.partial(back_kernel, sizes, seqs, heads, cuts),
        name="layer",
        out_shape=jax.ShapeDtypeStruct((rows, half * cb), BF16),
        in_specs=[anywhere() if 3 <= i < 10 else vmem() for i in range(len(args))],
        out_specs=vmem(),
        scratch_shapes=[
            pltpu.VMEM(query_up.shape, BF16),
            pltpu.VMEM(latent_up.shape, BF16),
            pltpu.VMEM((rows, 3 * third), BF16),
            pltpu.VMEM((C, rows, qw + kw), BF16),
            pltpu.VMEM((1, 128), F32),
            pltpu.VMEM((3, shard, third), BF16),
            pltpu.VMEM((depth, cb), BF16),
            pltpu.VMEM((3, n, shard, third), BF16),
            pltpu.VMEM((rows, kv_width), BF16),
            pltpu.VMEM((Z, rows, kv_width), BF16),
            pltpu.VMEM((lanes, HEAD, HEAD), BF16),
            pltpu.VMEM((lanes, HEAD, HEAD), BF16),
            pltpu.VMEM((rows, depth), BF16),
            pltpu.VMEM((n, depth, cb), BF16),
            pltpu.VMEM((n, rows, cb), BF16),
            pltpu.VMEM((half, rows, cb), BF16),
            pltpu.VMEM((2, rows, 128), F32),
            pltpu.SemaphoreType.DMA((16,)),
            pltpu.SemaphoreType.DMA((2, Z)),
            pltpu.SemaphoreType.DMA((2, lanes)),
        ]
        + Gather.scratch(Z, X) + Gather.scratch(Z, X) + [pltpu.SemaphoreType.DMA((6,))],
        compiler_params=pltpu.CompilerParams(
            collective_id=0, has_side_effects=True, vmem_limit_bytes=60 * 1024 * 1024
        ),
    )(*args)
    return result.reshape(seqs, count, half * cb)


def solution(mesh):
    sizes = tuple(mesh.shape[a] for a in ("grp", "sp", "fs", "tp"))
    return jax.shard_map(
        functools.partial(local, sizes),
        mesh=mesh,
        in_specs=(
            P(("grp", "fs"), "sp", None),
            P(),
            P(("sp", "fs"), "tp"),
            P(("sp", "fs"), "tp"),
            P(("sp", "fs"), "tp"),
            P(),
            P(),
            P(),
            P(),
            P(("sp", "fs"), None),
            P(("sp", "fs"), None),
            P(),
            P(),
            P(),
            P(None, "tp"),
            P(None, "tp"),
            P("tp", ("sp", "fs")),
            P("tp", ("sp", "fs")),
            P("tp"),
        ),
        out_specs=P(("grp", "fs"), "sp", "tp"),
        check_vma=False,
    )
```

profile of v0, /device:TPU:25, one launch (start us, length us, event | category | flops | bytes accessed | tf_op | source)
XLA Modules:
  0.0 118.1 jit_solution(11248274418224595623)
XLA Ops:
  0.0 0.1 pad.3.clone
  0.1 1.8 %maximum_maximum_fusion.small = bf16[128,2048]{1,0:T(8,128)(2,1)} fusion(bf16[32,2048]{1,0:T(8,128)(2,1)} %bitcast.13, bf16[8,2048]{1,0:T(8,128)(2,1)} %bitcast.14, bf16[8,2048]{1,0:T(8,128)(2,1)} %bitcast.15, bf16[128]{0:T(256)(128)(2,1)S(1)} %pad.3.clone), kind=kLoop, calls=%fused_computation | loop fusion | flops 2097152 | bytes 721152 | tf_op jit(solution)/shard_map/concatenate | solution.py:602
  1.9 114.5 %layer.1 = bf16[128,1024]{1,0:T(8,128)(2,1)} custom-call(bf16[128,2048]{1,0:T(8,128)(2,1)} %bitcast.12, f32[1,2048]{1,0:T(1,128)} %bitcast.16, bf16[128,2048]{1,0:T(8,128)(2,1)} %maximum_maximum_fusion.small, bf16[256,512]{1,0:T(8,128)(2,1)} %w_query.1, bf16[256,512]{1,0:T(8,128)(2,1)} %w_key.1, bf16[256,512]{1,0:T(8,128)(2,1)} %w_value.1, ...), custom_call_target="tpu_custom_call" | custom-call | tf_op jit(solution)/shard_map/layer/pallas_call | solution.py:615
  116.4 1.7 %copy.21 = bf16[2,64,1024]{2,1,0:T(8,128)(2,1)} copy(bf16[2,64,1024]{2,1,0:T(8,128)(2,1)} %bitcast.11) | data formatting | bytes 524288
  (1 shorter events, 0.0 us)
where the time goes:
time: 118 us
  Pallas kernels  114 us (97%)
  other arithmetic  1.84 us (2%)
  local copies, waits for them, and re-layouts  1.75 us (1%)
    pallas_call x1, Pallas kernels, local(): pl.pallas_call(functools.partial(back_kernel, sizes, seqs, heads, cuts),...  114 us

commit v1 on v0

--- a/solution.py
+++ b/solution.py
@@ -591,6 +591,13 @@
     Y, Z, X, C = sizes
     n = Z * X
     seqs, count, width = tokens.shape
+    if splits_by_heads(sizes, seqs, count, query_weight.shape, query_down.shape,
+                       latent_down.shape, query_up.shape, latent_up.shape):
+        return by_heads(
+            sizes, tokens, pre_gain, query_weight, key_weight, value_weight, beta_weight,
+            decay_weight, decay_rate, delta_gain, query_down, latent_down, rope_weight,
+            query_gain, latent_gain, query_up, latent_up, delta_out, latent_out, post_gain,
+        )
     rows = seqs * count
     qw = query_down.shape[1] // C
     kw = latent_down.shape[1] // C
@@ -648,6 +655,498 @@
     return result.reshape(seqs, count, half * cb)
 
 
+class Puts:
+    def __init__(self, sems):
+        self.sems, self.sent = sems, []
+
+    def put(self, cond, src, dst, recv, dev):
+        index = len(self.sent)
+
+        def make():
+            return pltpu.make_async_remote_copy(
+                src_ref=src, dst_ref=dst, send_sem=self.sems.at[index], recv_sem=recv,
+                device_id=dev, device_id_type=MESH,
+            )
+
+        when(cond, lambda: make().start())
+        self.sent.append((cond, make))
+
+    def drain(self):
+        for cond, make in self.sent:
+            when(cond, lambda make=make: make().wait_send())
+
+
+def landed(cond, ref, dummy, recv, c):
+    def wait():
+        pltpu.make_async_remote_copy(
+            src_ref=ref, dst_ref=ref, send_sem=dummy, recv_sem=recv,
+            device_id={"tp": c}, device_id_type=MESH,
+        ).wait_recv()
+
+    when(cond, wait)
+
+
+def heads_kernel(
+    sizes, seqs, cuts, tokens, pre_gain, w_beta, w_decay, w_rope, w_query, w_key, w_value,
+    w_qdown, w_kdown, w_delta, w_latent, qgain, kgain, w_qup, w_lup, rate_in, gain, post,
+    out, tok, beta_v, decay_v, rope_v, qup_v, lup_v, wown, wbuf, nbuf, ssel, qsel, turn_a, turn_b,
+    raw, sm, lat, hsrc, hbuf, own, buf, pbuf, rbuf, sq,
+    asem, wsend, wrecv, nsend, nrecv, lsend, lrecv, hsend, hrecv, osem, dummy,
+    send, recv, lsem, tsem,
+):
+    place = Place(sizes)
+    Z, X = place.Z, place.X
+    y, z, x, c = place.y, place.z, place.x, place.c
+    tile = 128
+    shard = wown.shape[1]
+    part = shard // 2
+    me = z * X + x
+    nk = w_kdown.shape[1] // tile
+    kblock = lax.rem(z, nk)
+    length = Z * BLOCK
+    count = seqs * length
+    width = nbuf.shape[3]
+    ncol = wown.shape[2]
+    loads = []
+
+    def load(src, dst, cond=True):
+        index = len(loads)
+
+        def make():
+            return pltpu.make_async_copy(src, dst, asem.at[index])
+
+        when(cond, lambda: make().start())
+        loads.append(make)
+        return index
+
+    first = []
+    for d in range(Z):
+        for i, w in enumerate((w_query, w_key, w_value)):
+            at = wown.at[d, :, pl.ds(i * tile, tile)]
+            first.append(load(w.at[:, pl.ds(d * tile, tile)], at))
+        at = wown.at[d, :, pl.ds(3 * tile, tile)]
+        index = load(w_qdown.at[:, pl.ds(d * tile, tile)], at, c == 0)
+        first.append(index)
+        kd = d % nk
+
+        def other(kd=kd, at=at, index=index):
+            pltpu.make_async_copy(
+                w_kdown.at[:, pl.ds(kd * tile, tile)], at, asem.at[index]
+            ).start()
+
+        when(c == 1, other)
+    tok_at = load(tokens, tok)
+    rest = [load(a, b) for a, b in (
+        (w_beta, beta_v), (w_decay, decay_v), (w_rope, rope_v), (w_qup, qup_v), (w_lup, lup_v),
+    )]
+    upper = w_delta.shape[0]
+    outs = [load(w_delta, own.at[pl.ds(0, upper)]),
+            load(w_latent, own.at[pl.ds(upper, w_latent.shape[0])])]
+
+    barrier = pltpu.get_barrier_semaphore()
+    peers = [{"sp": lax.rem(z + k, Z)} for k in range(1, Z)]
+    peers += [{"fs": 1 - x}, {"grp": 1 - y}, {"fs": 1 - x, "grp": 1 - y}, {"tp": 1 - c}]
+    for dev in peers:
+        pl.semaphore_signal(barrier, inc=1, device_id=dev, device_id_type=MESH)
+    pl.semaphore_wait(barrier, len(peers))
+
+    for index in first:
+        loads[index]().wait()
+    W, N, L, H = Puts(wsend), Puts(nsend), Puts(lsend), Puts(hsend)
+    mine = pl.ds(pl.multiple_of(y * part, part), part)
+    yours = pl.ds(pl.multiple_of((1 - y) * part, part), part)
+    for k in range(1, Z):
+        to = lax.rem(z + k, Z)
+        W.put(True, wown.at[to, mine], wbuf.at[me, mine], wrecv.at[me, y], {"sp": to})
+    W.put(True, wown.at[z], wbuf.at[me], wrecv.at[me, 0], {"fs": 1 - x})
+    keep_own = pltpu.make_async_copy(wown.at[z], wbuf.at[me], osem.at[0])
+    keep_own.start()
+    loads[tok_at]().wait()
+    for b in range(seqs):
+        t = tok[b * BLOCK : (b + 1) * BLOCK].astype(F32)
+        scale = lax.rsqrt(jnp.mean(t * t, axis=-1, keepdims=True) + NORM_EPS)
+        nbuf[b, z] = (t * scale * pre_gain[...]).astype(BF16)
+    for sign in (1, -1):
+        nxt = z + sign
+        N.put(jnp.logical_and(nxt >= 0, nxt < Z), nbuf.at[c, z], nbuf.at[c, z],
+              nrecv.at[c, z], {"sp": nxt})
+
+    for index in rest:
+        loads[index]().wait()
+    lane = lax.broadcasted_iota(jnp.int32, (length, tile), 1)
+    row = lax.broadcasted_iota(jnp.int32, (length, tile), 0)
+    half_turn = ROPE // 2
+    step = (lane % half_turn).astype(F32)
+    angle = row.astype(F32) * jnp.exp(step * (-2.0 * math.log(ROPE_THETA) / ROPE))
+    turning = (lane >= NOPE) & (lane < NOPE + ROPE)
+    turn_a[...] = jnp.where(lane < NOPE, 1.0, jnp.where(turning, jnp.cos(angle), 0.0))
+    sin_t = jnp.sin(angle)
+    turn_b[...] = jnp.where(turning, jnp.where(lane < NOPE + half_turn, -sin_t, sin_t), 0.0)
+
+    def pick(cond):
+        return jnp.where(cond, 1.0, 0.0).astype(BF16)
+
+    head = c * w_query.shape[1] // HEAD + z
+    nb = w_beta.shape[1]
+    r8 = lax.broadcasted_iota(jnp.int32, (nb, 2 * tile), 0)
+    l8 = lax.broadcasted_iota(jnp.int32, (nb, 2 * tile), 1)
+    r32 = lax.broadcasted_iota(jnp.int32, (ROPE, 2 * tile), 0)
+    l32 = lax.broadcasted_iota(jnp.int32, (ROPE, 2 * tile), 1)
+    turned_lane = jnp.where(l32 < tile, r32 + NOPE, (r32 + half_turn) % ROPE + NOPE + tile)
+    ssel[...] = (
+        dot(beta_v[...], pick((r8 == head) & (l8 == 0)))
+        + dot(decay_v[...], pick((r8 == head) & (l8 == 1)))
+        + dot(rope_v[...], pick(l32 == turned_lane))
+    ).astype(BF16)
+    per = NOPE + ROPE
+    lh = w_qup.shape[1] // per // Z
+    qd = lax.broadcasted_iota(jnp.int32, (w_qup.shape[1], tile), 1)
+    qs = lax.broadcasted_iota(jnp.int32, (w_qup.shape[1], tile), 0)
+    swapped = jnp.where(qd < NOPE, qd, NOPE + (qd - NOPE + half_turn) % ROPE)
+    for j in range(lh):
+        base = (z * lh + j) * per
+        qsel[:, j * tile : (j + 1) * tile] = dot(
+            qup_v[...], pick((qd < per) & (qs == base + qd))
+        ).astype(BF16)
+        qsel[:, (lh + j) * tile : (lh + j + 1) * tile] = dot(
+            qup_v[...], pick((qd >= NOPE) & (qd < per) & (qs == base + swapped))
+        ).astype(BF16)
+
+    for index in outs:
+        loads[index]().wait()
+    g = Gather(
+        place,
+        lambda p: own.at[pl.ds(cuts[p], cuts[p + 1] - cuts[p])],
+        lambda p, s: buf.at[s, pl.ds(cuts[p], cuts[p + 1] - cuts[p])],
+        send, recv, lsem,
+    )
+
+    def wait_w(zz, xx, yy, rows):
+        slot = zz * X + xx
+        landed(True, wbuf.at[slot, rows], dummy.at[0], wrecv.at[slot, yy], c)
+
+    for k in range(1, Z):
+        zz = lax.rem(z - k + Z, Z)
+        slot = zz * X + x
+        wait_w(zz, x, y, mine)
+        for dev in ({"fs": 1 - x}, {"grp": 1 - y}, {"fs": 1 - x, "grp": 1 - y}):
+            ref = wbuf.at[slot, mine]
+            W.put(True, ref, ref, wrecv.at[slot, y], dev)
+        for sign in (1, -1):
+            zz = z - sign * k
+            ok = jnp.logical_and(zz >= 0, zz < Z)
+            nxt = z + sign
+            ref = nbuf.at[c, zz]
+            landed(ok, ref, dummy.at[1], nrecv.at[c, zz], c)
+            N.put(both(ok, jnp.logical_and(nxt >= 0, nxt < Z)), ref, ref, nrecv.at[c, zz],
+                  {"sp": nxt})
+            N.put(ok, ref, ref, nrecv.at[c, zz], {"tp": 1 - c})
+        if k == max(1, Z - 2):
+            g.start_along()
+    g.start_across()
+    for k in range(1, Z):
+        zz = lax.rem(z - k + Z, Z)
+        wait_w(zz, x, 1 - y, yours)
+        wait_w(zz, 1 - x, y, mine)
+        wait_w(zz, 1 - x, 1 - y, yours)
+    slot = z * X + 1 - x
+    landed(True, wbuf.at[slot], dummy.at[0], wrecv.at[slot, 0], c)
+    keep_own.wait()
+    for k in range(1, Z):
+        zz = lax.rem(z - k + Z, Z)
+        landed(True, nbuf.at[1 - c, zz], dummy.at[1], nrecv.at[1 - c, zz], c)
+
+    lslot = (1 - c) * z + c * (Z + kblock)
+    for b in range(seqs):
+        at = slice(b * length, (b + 1) * length)
+        normed = nbuf[b].reshape(length, width)
+        pr = dot(normed, wbuf[...].reshape(width, ncol)).astype(BF16)
+        lat[lslot, at] = pr[:, 3 * tile :]
+        raw[at] = pr[:, : 3 * tile]
+        sm[at] = dot(normed, ssel[...])
+
+    def latput(cond, slot, dev):
+        L.put(cond, lat.at[slot], lat.at[slot], lrecv.at[slot], dev)
+
+    for k in range(1, Z):
+        latput(c == 0, z, {"sp": lax.rem(z + k, Z)})
+    pair = z - kblock
+    for k in range(1, nk):
+        latput(c == 1, Z + kblock, {"sp": pair + lax.rem(kblock + k, nk)})
+    latput(True, lslot, {"tp": 1 - c})
+    g.step(1)
+
+    ri = lax.broadcasted_iota(jnp.int32, (BLOCK, BLOCK), 0)
+    ci = lax.broadcasted_iota(jnp.int32, (BLOCK, BLOCK), 1)
+    strict = ri > ci
+    causal = ri >= ci
+    eye = jnp.where(ri == ci, 1.0, 0.0).astype(F32)
+    tri = jnp.where(causal, 1.0, 0.0).astype(F32)
+    units = [(b, n) for b in range(seqs) for n in range(Z)]
+    lane1 = lax.broadcasted_iota(jnp.int32, (1, nb), 1)
+    rate = jnp.sum(jnp.where(lane1 == head, rate_in[...], 0.0), axis=-1, keepdims=True)
+    pre_b = sm[:, 0:1]
+    pre_d = sm[:, 1:2]
+    beta_all = jax.nn.sigmoid(pre_b)
+    log_a = -rate * (jnp.maximum(pre_d, 0.0) + jnp.log1p(jnp.exp(-jnp.abs(pre_d))))
+    blane = lax.broadcasted_iota(jnp.int32, (BLOCK, tile), 1)
+    spread_a = jnp.zeros((BLOCK, tile), F32)
+    for u in range(len(units)):
+        spread_a = jnp.where(blane == u, log_a[u * BLOCK : (u + 1) * BLOCK], spread_a)
+    gates = dot(tri, spread_a, HIGHEST)
+    gates_t = gates.T
+    terms = []
+    for u in range(len(units)):
+        at = slice(u * BLOCK, (u + 1) * BLOCK)
+
+        def act(i):
+            v = raw[at, i * tile : (i + 1) * tile].astype(F32)
+            return v * jax.nn.sigmoid(v)
+
+        def unit(v):
+            return v * lax.rsqrt(jnp.sum(v * v, axis=-1, keepdims=True) + NORM_EPS)
+
+        q = unit(act(0)) * HEAD ** (-0.5)
+        k = unit(act(1))
+        v = act(2)
+        beta = beta_all[at]
+        gcol = gates[:, u : u + 1]
+        grow = gates_t[u : u + 1, :]
+        glast = gates[BLOCK - 1 : BLOCK, u : u + 1]
+        gap = gcol - grow
+        decay = jnp.where(causal, jnp.exp(jnp.where(causal, gap, 0.0)), 0.0)
+        ks = k * beta
+        low = jnp.where(strict, dot_t(ks, k, HIGHEST) * decay, 0.0)
+        scores = dot_t(q.astype(BF16), k.astype(BF16)) * decay
+        eg = jnp.exp(gcol)
+        terms.append([low, scores, v * beta, ks * eg, q * eg, k * jnp.exp(glast - gcol),
+                      jnp.exp(glast)])
+    every = range(len(units))
+    inv = [eye - jnp.where((ri // 2 == ci // 2), terms[i][0], 0.0) for i in every]
+    size = 2
+    while size < BLOCK:
+        joint = (ri // (2 * size) == ci // (2 * size)) & (ri // size != ci // size)
+        mids = [dot(jnp.where(joint, terms[i][0], 0.0), inv[i], HIGHEST) for i in every]
+        inv = [inv[i] - dot(inv[i], mids[i], HIGHEST) for i in every]
+        size *= 2
+    inv = [m.astype(BF16) for m in inv]
+    nv = [dot(inv[i], terms[i][2].astype(BF16)) for i in every]
+    kw = [dot(inv[i], terms[i][3].astype(BF16)).astype(BF16) for i in every]
+    g.cross_step(0)
+    if Z > 2:
+        g.step(2)
+    state = [None] * seqs
+    for n in range(Z):
+        for b in range(seqs):
+            i = b * Z + n
+            _, scores, _, _, qd_, kd_, factor = terms[i]
+            corrected = nv[i]
+            if n:
+                s_in = state[b].astype(BF16)
+                corrected = corrected - dot(kw[i], s_in)
+            o = dot(scores.astype(BF16), corrected.astype(BF16))
+            if n:
+                o = o + dot(qd_.astype(BF16), s_in)
+            grown = t_dot(kd_.astype(BF16), corrected.astype(BF16))
+            state[b] = state[b] * factor + grown if n else grown
+            o = o * lax.rsqrt(jnp.mean(o * o, axis=-1, keepdims=True) + NORM_EPS) * gain[...]
+            hsrc[0, n, b * BLOCK : (b + 1) * BLOCK] = o.astype(BF16)
+
+    def give(kind):
+        hbuf[kind, z] = hsrc[kind, z]
+        for k in range(1, Z):
+            to = lax.rem(z + k, Z)
+            H.put(True, hsrc.at[kind, to], hbuf.at[kind, z], hrecv.at[kind, z], {"sp": to})
+
+    give(0)
+    for k in range(1, Z):
+        zz = lax.rem(z - k + Z, Z)
+        landed(c == 0, lat.at[zz], dummy.at[2], lrecv.at[zz], c)
+        latput(c == 0, zz, {"tp": 1 - c})
+    for k in range(1, nk):
+        slot = Z + lax.rem(kblock + k, nk)
+        landed(c == 1, lat.at[slot], dummy.at[2], lrecv.at[slot], c)
+        latput(c == 1, slot, {"tp": 1 - c})
+    g.cross_step(1)
+    for k in range(3, Z):
+        g.step(k)
+        if k < Z - 1:
+            g.cross_step(k - 1)
+    for s in range(Z):
+        landed(c == 1, lat.at[s], dummy.at[2], lrecv.at[s], c)
+    for s in range(Z, Z + nk):
+        landed(c == 0, lat.at[s], dummy.at[2], lrecv.at[s], c)
+
+    scale = per ** (-0.5)
+    la = lax.broadcasted_iota(jnp.int32, (length, length), 1) // BLOCK
+    lb = lax.broadcasted_iota(jnp.int32, (length, length), 0) // BLOCK
+    allowed = la <= lb
+    lcol = pl.ds(pl.multiple_of(z * lh * tile, lh * tile), lh * tile)
+
+    def normed_parts(slots, at, g_):
+        parts = [lat[s, at].astype(F32) for s in slots]
+        squares = sum(jnp.sum(p * p, axis=-1, keepdims=True) for p in parts)
+        factor = lax.rsqrt(squares / (len(parts) * tile) + NORM_EPS)
+        return jnp.concatenate(
+            [(p * factor * g_[:, i * tile : (i + 1) * tile]).astype(BF16)
+             for i, p in enumerate(parts)], axis=1
+        )
+
+    for b in range(seqs):
+        at = slice(b * length, (b + 1) * length)
+        ta, tb = turn_a[...], turn_b[...]
+        qn = normed_parts(range(Z), at, qgain)
+        kn = normed_parts(range(Z, Z + nk), at, kgain)
+        qa = dot(qn, qsel[...]).astype(BF16).astype(F32)
+        ka = dot(kn, lup_v[:, lcol]).astype(BF16)
+        rope = sm[at].astype(BF16).astype(F32)
+        turned = (rope[:, :tile] * ta + rope[:, tile:] * tb).astype(BF16)
+        outs_ = []
+        for j in range(lh):
+            qf = (qa[:, j * tile : (j + 1) * tile] * ta
+                  + qa[:, (lh + j) * tile : (lh + j + 1) * tile] * tb).astype(BF16)
+            kj = ka[:, j * tile : (j + 1) * tile]
+            kf = jnp.where(lane < NOPE, kj, turned)
+            s = jnp.where(allowed, dot_t(qf, kf) * scale, -jnp.inf)
+            w = jnp.exp(s - jnp.max(s, axis=-1, keepdims=True))
+            o = dot(w.astype(BF16), kj) / jnp.sum(w, axis=-1, keepdims=True)
+            outs_.append(o)
+        both_ = jnp.where(lane < VDIM, pltpu.roll(outs_[0], VDIM, 1), outs_[1]).astype(BF16)
+        for n in range(Z):
+            hsrc[1, n, b * BLOCK : (b + 1) * BLOCK] = both_[n * BLOCK : (n + 1) * BLOCK]
+    give(1)
+    if Z > 3:
+        g.cross_step(Z - 2)
+    g.finish()
+    for kind in range(2):
+        for k in range(1, Z):
+            zz = lax.rem(z - k + Z, Z)
+            landed(True, hbuf.at[kind, zz], dummy.at[2], hrecv.at[kind, zz], c)
+    hv = jnp.concatenate([hbuf[kind, s] for kind in range(2) for s in range(Z)], axis=1)
+    n = buf.shape[0]
+    half = n // 2
+    rows = hv.shape[0]
+
+    def piece(s, carry):
+        pbuf[s] = dot(hv, buf[s]).astype(BF16)
+        return carry
+
+    lax.fori_loop(0, n, piece, 0)
+    peer = 1 - c
+    copy = pltpu.make_async_remote_copy(
+        src_ref=pbuf.at[pl.ds(peer * half, half)], dst_ref=rbuf, send_sem=tsem.at[0],
+        recv_sem=tsem.at[1], device_id={"tp": peer}, device_id_type=MESH,
+    )
+    copy.start()
+    for p in (W, N, L, H, g):
+        p.drain()
+    copy.wait()
+    total = jnp.zeros((rows, 1), F32)
+    mixed = []
+    for s in range(half):
+        m = pbuf[c * half + s].astype(F32) + rbuf[s].astype(F32)
+        mixed.append(m)
+        total = total + jnp.sum(m * m, axis=-1, keepdims=True)
+    sq[0] = jnp.broadcast_to(total, sq.shape[1:])
+    squares = pltpu.make_async_remote_copy(
+        src_ref=sq.at[0], dst_ref=sq.at[1], send_sem=tsem.at[2], recv_sem=tsem.at[3],
+        device_id={"tp": peer}, device_id_type=MESH,
+    )
+    squares.start()
+    squares.wait()
+    total = total + sq[1][:, :1]
+    cb = buf.shape[2]
+    norm = lax.rsqrt(total / (n * cb) + NORM_EPS)
+    for s in range(half):
+        out[:, s * cb : (s + 1) * cb] = (mixed[s] * norm * post[s]).astype(BF16)
+
+
+def splits_by_heads(sizes, seqs, count, qw, qd, kd, qup, lup):
+    Y, Z, X, C = sizes
+    nk = kd[1] // 128
+    return (
+        Y == 2 and X == 2 and C == 2 and seqs == C and count == BLOCK and qw[1] == Z * HEAD
+        and qd[1] == Z * 128 and kd[1] == nk * 128 and Z % nk == 0
+        and qup[1] == Z * 2 * (NOPE + ROPE) and lup[1] == Z * 2 * (NOPE + VDIM)
+    )
+
+
+def by_heads(sizes, *arrays):
+    (tokens, pre_gain, query_weight, key_weight, value_weight, beta_weight, decay_weight,
+     decay_rate, delta_gain, query_down, latent_down, rope_weight, query_gain, latent_gain,
+     query_up, latent_up, delta_out, latent_out, post_gain) = arrays
+    Y, Z, X, C = sizes
+    n = Z * X
+    seqs, count, width = tokens.shape
+    rows = seqs * count
+    shard = query_weight.shape[0]
+    nk = latent_down.shape[1] // 128
+    cb = delta_out.shape[1]
+    depth = delta_out.shape[0] + latent_out.shape[0]
+    cuts = (0, depth * 7 // 16, depth * 14 // 16, depth)
+    half = n // 2
+    lh = query_up.shape[1] // (NOPE + ROPE) // Z
+    total = rows * Z
+    ncol = 4 * 128
+    args = (
+        tokens.reshape(rows, width), pre_gain.reshape(1, width),
+        beta_weight, decay_weight, rope_weight,
+        query_weight, key_weight, value_weight, query_down, latent_down, delta_out, latent_out,
+        query_gain.reshape(1, -1), latent_gain.reshape(1, -1), query_up, latent_up,
+        decay_rate.reshape(1, -1), delta_gain.reshape(1, HEAD), post_gain.reshape(half, 1, cb),
+    )
+    hbm = (0, 2, 3, 4, 5, 6, 7, 8, 9, 10, 11, 14, 15)
+    DMA = pltpu.SemaphoreType.DMA
+    result = pl.pallas_call(
+        functools.partial(heads_kernel, sizes, seqs, cuts),
+        name="layer",
+        out_shape=jax.ShapeDtypeStruct((rows, half * cb), BF16),
+        in_specs=[anywhere() if i in hbm else vmem() for i in range(len(args))],
+        out_specs=vmem(),
+        scratch_shapes=[
+            pltpu.VMEM((rows, width), BF16),
+            pltpu.VMEM(beta_weight.shape, BF16),
+            pltpu.VMEM(decay_weight.shape, BF16),
+            pltpu.VMEM(rope_weight.shape, BF16),
+            pltpu.VMEM(query_up.shape, BF16),
+            pltpu.VMEM(latent_up.shape, BF16),
+            pltpu.VMEM((Z, shard, ncol), BF16),
+            pltpu.VMEM((n, shard, ncol), BF16),
+            pltpu.VMEM((seqs, Z, BLOCK, width), BF16),
+            pltpu.VMEM((width, 256), BF16),
+            pltpu.VMEM((query_up.shape[0], 2 * lh * 128), BF16),
+            pltpu.VMEM((Z * BLOCK, 128), F32),
+            pltpu.VMEM((Z * BLOCK, 128), F32),
+            pltpu.VMEM((total, 384), BF16),
+            pltpu.VMEM((total, 256), F32),
+            pltpu.VMEM((Z + nk, total, 128), BF16),
+            pltpu.VMEM((2, Z, rows, 128), BF16),
+            pltpu.VMEM((2, Z, rows, 128), BF16),
+            pltpu.VMEM((depth, cb), BF16),
+            pltpu.VMEM((n, depth, cb), BF16),
+            pltpu.VMEM((n, rows, cb), BF16),
+            pltpu.VMEM((half, rows, cb), BF16),
+            pltpu.VMEM((2, rows, 128), F32),
+            DMA((4 * Z + 8,)),
+            DMA((4 * Z,)),
+            DMA((n, 2)),
+            DMA((2 + 4 * Z,)),
+            DMA((seqs, Z)),
+            DMA((2 * Z + 2 * nk,)),
+            DMA((Z + nk,)),
+            DMA((2 * Z,)),
+            DMA((2, Z)),
+            DMA((1,)),
+            DMA((3,)),
+        ]
+        + Gather.scratch(Z, X) + [DMA((6,))],
+        compiler_params=pltpu.CompilerParams(
+            collective_id=0, has_side_effects=True, vmem_limit_bytes=60 * 1024 * 1024
+        ),
+    )(*args)
+    return result.reshape(seqs, count, half * cb)
+
+
 def solution(mesh):
     sizes = tuple(mesh.shape[a] for a in ("grp", "sp", "fs", "tp"))
     return jax.shard_map(

time: 118 us -> 92.4 us (0.78)
  the two profiles are of different devices: /device:TPU:25 before, /device:TPU:0 now
where the time goes in v1:
time: 92.4 us; the launch traced here: 92.1 us
  Pallas kernels  86.7 us (94%)
  local copies, waits for them, and re-layouts  5.45 us (6%)
    pallas_call x1, Pallas kernels, by_heads(): pl.pallas_call(functools.partial(heads_kernel, sizes, seqs, cuts), name='...  86.7 us
    unnamed x8, local copies, waits for them, and re-layouts  5.45 us

profile of v1, /device:TPU:0, one launch (start us, length us, event | category | flops | bytes accessed | tf_op | source)
XLA Modules:
  0.0 92.1 jit_solution(16972262242740618865)
XLA Ops:
  0.0 0.0 copy-start.1
  0.0 1.8 %copy.20.w_beta = bf16[2048,8]{1,0:T(8,128)(2,1)} copy(bf16[2048,8]{0,1:T(8,128)(2,1)} %param.24) | data formatting | bytes 65536 | tf_op args[5]
  1.8 0.0 copy-done.1
  1.8 0.0 copy-start
  1.8 1.0 %copy.21.w_decay = bf16[2048,8]{1,0:T(8,128)(2,1)} copy(bf16[2048,8]{0,1:T(8,128)(2,1)S(1)} %copy-done.1) | data formatting | bytes 65536 | tf_op args[6]
  2.8 0.0 copy-done
  2.8 1.0 %copy.22.w_rope = bf16[2048,32]{1,0:T(8,128)(2,1)} copy(bf16[2048,32]{0,1:T(8,128)(2,1)S(1)} %copy-done) | data formatting | bytes 262144 | tf_op args[11]
  3.8 86.7 %layer.1 = bf16[128,1024]{1,0:T(8,128)(2,1)} custom-call(bf16[128,2048]{1,0:T(8,128)(2,1)} %bitcast.9, f32[1,2048]{1,0:T(1,128)} %bitcast.10, bf16[2048,8]{1,0:T(8,128)(2,1)} %copy.20.w_beta, bf16[2048,8]{1,0:T(8,128)(2,1)} %copy.21.w_decay, bf16[2048,32]{1,0:T(8,128)(2,1)} %copy.22.w_rope, bf16[256,512]{1,0:T(8,128)(2,1)} %w_query.1, ...), custom_call_target="tpu_custom_call" | custom-call | tf_op jit(solution)/shard_map/layer/pallas_call | solution.py:1100
  90.5 1.7 %copy.24 = bf16[2,64,1024]{2,1,0:T(8,128)(2,1)} copy(bf16[2,64,1024]{2,1,0:T(8,128)(2,1)} %bitcast.8) | data formatting | bytes 524288
Async XLA Ops:
  0.0 1.8 %copy-start.1 = (bf16[2048,8]{0,1:T(8,128)(2,1)S(1)}, bf16[2048,8]{0,1:T(8,128)(2,1)}, u32[]{:S(2)}) copy-start(bf16[2048,8]{0,1:T(8,128)(2,1)} %param.25) | copy-start | bytes 98308
  1.8 1.0 %copy-start = (bf16[2048,32]{0,1:T(8,128)(2,1)S(1)}, bf16[2048,32]{0,1:T(8,128)(2,1)}, u32[]{:S(2)}) copy-start(bf16[2048,32]{0,1:T(8,128)(2,1)} %param.30) | copy-start | bytes 393220

commit v2 on v1

--- a/solution.py
+++ b/solution.py
@@ -592,7 +592,8 @@
     n = Z * X
     seqs, count, width = tokens.shape
     if splits_by_heads(sizes, seqs, count, query_weight.shape, query_down.shape,
-                       latent_down.shape, query_up.shape, latent_up.shape):
+                       latent_down.shape, query_up.shape, latent_up.shape, delta_out.shape,
+                       latent_out.shape):
         return by_heads(
             sizes, tokens, pre_gain, query_weight, key_weight, value_weight, beta_weight,
             decay_weight, decay_rate, delta_gain, query_down, latent_down, rope_weight,
@@ -687,12 +688,12 @@
 
 
 def heads_kernel(
-    sizes, seqs, cuts, tokens, pre_gain, w_beta, w_decay, w_rope, w_query, w_key, w_value,
+    sizes, seqs, tokens, pre_gain, w_beta, w_decay, w_rope, w_query, w_key, w_value,
     w_qdown, w_kdown, w_delta, w_latent, qgain, kgain, w_qup, w_lup, rate_in, gain, post,
     out, tok, beta_v, decay_v, rope_v, qup_v, lup_v, wown, wbuf, nbuf, ssel, qsel, turn_a, turn_b,
-    raw, sm, lat, hsrc, hbuf, own, buf, pbuf, rbuf, sq,
-    asem, wsend, wrecv, nsend, nrecv, lsend, lrecv, hsend, hrecv, osem, dummy,
-    send, recv, lsem, tsem,
+    raw, sm, lat, hsrc, hbuf, obuf, pbuf, rbuf, sq,
+    asem, wsend, wrecv, nsend, nrecv, lsend, lrecv, hsend, hrecv, osend, orecv, psend, precv,
+    ksem, dummy, tsem,
 ):
     place = Place(sizes)
     Z, X = place.Z, place.X
@@ -707,6 +708,12 @@
     count = seqs * length
     width = nbuf.shape[3]
     ncol = wown.shape[2]
+    barrier = pltpu.get_barrier_semaphore()
+    peers = [{"sp": lax.rem(z + k, Z)} for k in range(1, Z)]
+    peers += [{"fs": 1 - x}, {"grp": 1 - y}, {"fs": 1 - x, "grp": 1 - y}, {"tp": 1 - c},
+              {"fs": 1 - x, "tp": 1 - c}]
+    for dev in peers:
+        pl.semaphore_signal(barrier, inc=1, device_id=dev, device_id_type=MESH)
     loads = []
 
     def load(src, dst, cond=True):
@@ -740,26 +747,22 @@
         (w_beta, beta_v), (w_decay, decay_v), (w_rope, rope_v), (w_qup, qup_v), (w_lup, lup_v),
     )]
     upper = w_delta.shape[0]
-    outs = [load(w_delta, own.at[pl.ds(0, upper)]),
-            load(w_latent, own.at[pl.ds(upper, w_latent.shape[0])])]
-
-    barrier = pltpu.get_barrier_semaphore()
-    peers = [{"sp": lax.rem(z + k, Z)} for k in range(1, Z)]
-    peers += [{"fs": 1 - x}, {"grp": 1 - y}, {"fs": 1 - x, "grp": 1 - y}, {"tp": 1 - c}]
-    for dev in peers:
-        pl.semaphore_signal(barrier, inc=1, device_id=dev, device_id_type=MESH)
+    outs = [load(w_delta, obuf.at[z, pl.ds(0, upper)]),
+            load(w_latent, obuf.at[z, pl.ds(upper, w_latent.shape[0])])]
+
     pl.semaphore_wait(barrier, len(peers))
 
     for index in first:
         loads[index]().wait()
     W, N, L, H = Puts(wsend), Puts(nsend), Puts(lsend), Puts(hsend)
+    O, R = Puts(osend), Puts(psend)
     mine = pl.ds(pl.multiple_of(y * part, part), part)
     yours = pl.ds(pl.multiple_of((1 - y) * part, part), part)
     for k in range(1, Z):
         to = lax.rem(z + k, Z)
         W.put(True, wown.at[to, mine], wbuf.at[me, mine], wrecv.at[me, y], {"sp": to})
     W.put(True, wown.at[z], wbuf.at[me], wrecv.at[me, 0], {"fs": 1 - x})
-    keep_own = pltpu.make_async_copy(wown.at[z], wbuf.at[me], osem.at[0])
+    keep_own = pltpu.make_async_copy(wown.at[z], wbuf.at[me], ksem.at[0])
     keep_own.start()
     loads[tok_at]().wait()
     for b in range(seqs):
@@ -787,16 +790,16 @@
         return jnp.where(cond, 1.0, 0.0).astype(BF16)
 
     head = c * w_query.shape[1] // HEAD + z
-    nb = w_beta.shape[1]
-    r8 = lax.broadcasted_iota(jnp.int32, (nb, 2 * tile), 0)
-    l8 = lax.broadcasted_iota(jnp.int32, (nb, 2 * tile), 1)
-    r32 = lax.broadcasted_iota(jnp.int32, (ROPE, 2 * tile), 0)
-    l32 = lax.broadcasted_iota(jnp.int32, (ROPE, 2 * tile), 1)
+    nb = w_beta.shape[0]
+    r8 = lax.broadcasted_iota(jnp.int32, (2 * tile, nb), 1)
+    l8 = lax.broadcasted_iota(jnp.int32, (2 * tile, nb), 0)
+    r32 = lax.broadcasted_iota(jnp.int32, (2 * tile, ROPE), 1)
+    l32 = lax.broadcasted_iota(jnp.int32, (2 * tile, ROPE), 0)
     turned_lane = jnp.where(l32 < tile, r32 + NOPE, (r32 + half_turn) % ROPE + NOPE + tile)
     ssel[...] = (
-        dot(beta_v[...], pick((r8 == head) & (l8 == 0)))
-        + dot(decay_v[...], pick((r8 == head) & (l8 == 1)))
-        + dot(rope_v[...], pick(l32 == turned_lane))
+        dot(pick((r8 == head) & (l8 == 0)), beta_v[...])
+        + dot(pick((r8 == head) & (l8 == 1)), decay_v[...])
+        + dot(pick(l32 == turned_lane), rope_v[...])
     ).astype(BF16)
     per = NOPE + ROPE
     lh = w_qup.shape[1] // per // Z
@@ -814,12 +817,27 @@
 
     for index in outs:
         loads[index]().wait()
-    g = Gather(
-        place,
-        lambda p: own.at[pl.ds(cuts[p], cuts[p + 1] - cuts[p])],
-        lambda p, s: buf.at[s, pl.ds(cuts[p], cuts[p + 1] - cuts[p])],
-        send, recv, lsem,
-    )
+    obl = upper
+    omine = pl.ds(pl.multiple_of(y * obl, obl), obl)
+    oyours = pl.ds(pl.multiple_of((1 - y) * obl, obl), obl)
+
+    def out_send(dist):
+        for sign in (1, -1):
+            to = z + sign * dist
+            ref = obuf.at[z, omine]
+            O.put(jnp.logical_and(to >= 0, to < Z), ref, ref, orecv.at[z, y], {"sp": to})
+
+    def out_pass(dist):
+        for sign in (1, -1):
+            zz = z - sign * dist
+            ok = jnp.logical_and(zz >= 0, zz < Z)
+            nxt = z + sign
+            ref = obuf.at[zz, omine]
+            landed(ok, ref, dummy.at[0], orecv.at[zz, y], c)
+            if dist >= 2:
+                O.put(both(ok, jnp.logical_and(nxt >= 0, nxt < Z)), ref, ref,
+                      orecv.at[zz, y], {"sp": nxt})
+            O.put(ok, ref, ref, orecv.at[zz, y], {"grp": 1 - y})
 
     def wait_w(zz, xx, yy, rows):
         slot = zz * X + xx
@@ -842,8 +860,7 @@
                   {"sp": nxt})
             N.put(ok, ref, ref, nrecv.at[c, zz], {"tp": 1 - c})
         if k == max(1, Z - 2):
-            g.start_along()
-    g.start_across()
+            out_send(1)
     for k in range(1, Z):
         zz = lax.rem(z - k + Z, Z)
         wait_w(zz, x, 1 - y, yours)
@@ -863,7 +880,7 @@
         pr = dot(normed, wbuf[...].reshape(width, ncol)).astype(BF16)
         lat[lslot, at] = pr[:, 3 * tile :]
         raw[at] = pr[:, : 3 * tile]
-        sm[at] = dot(normed, ssel[...])
+        sm[at] = dot_t(normed, ssel[...])
 
     def latput(cond, slot, dev):
         L.put(cond, lat.at[slot], lat.at[slot], lrecv.at[slot], dev)
@@ -874,7 +891,7 @@
     for k in range(1, nk):
         latput(c == 1, Z + kblock, {"sp": pair + lax.rem(kblock + k, nk)})
     latput(True, lslot, {"tp": 1 - c})
-    g.step(1)
+    out_send(2)
 
     ri = lax.broadcasted_iota(jnp.int32, (BLOCK, BLOCK), 0)
     ci = lax.broadcasted_iota(jnp.int32, (BLOCK, BLOCK), 1)
@@ -932,9 +949,6 @@
     inv = [m.astype(BF16) for m in inv]
     nv = [dot(inv[i], terms[i][2].astype(BF16)) for i in every]
     kw = [dot(inv[i], terms[i][3].astype(BF16)).astype(BF16) for i in every]
-    g.cross_step(0)
-    if Z > 2:
-        g.step(2)
     state = [None] * seqs
     for n in range(Z):
         for b in range(seqs):
@@ -953,10 +967,18 @@
             hsrc[0, n, b * BLOCK : (b + 1) * BLOCK] = o.astype(BF16)
 
     def give(kind):
-        hbuf[kind, z] = hsrc[kind, z]
         for k in range(1, Z):
             to = lax.rem(z + k, Z)
-            H.put(True, hsrc.at[kind, to], hbuf.at[kind, z], hrecv.at[kind, z], {"sp": to})
+            H.put(True, hsrc.at[kind, to], hbuf.at[x, kind, z], hrecv.at[x, kind, z], {"sp": to})
+        hbuf[x, kind, z] = hsrc[kind, z]
+        H.put(True, hsrc.at[kind, z], hbuf.at[x, kind, z], hrecv.at[x, kind, z], {"fs": 1 - x})
+
+    def pass_heads(kind):
+        for k in range(1, Z):
+            zz = lax.rem(z - k + Z, Z)
+            ref = hbuf.at[x, kind, zz]
+            landed(True, ref, dummy.at[2], hrecv.at[x, kind, zz], c)
+            H.put(True, ref, ref, hrecv.at[x, kind, zz], {"fs": 1 - x})
 
     give(0)
     for k in range(1, Z):
@@ -967,11 +989,6 @@
         slot = Z + lax.rem(kblock + k, nk)
         landed(c == 1, lat.at[slot], dummy.at[2], lrecv.at[slot], c)
         latput(c == 1, slot, {"tp": 1 - c})
-    g.cross_step(1)
-    for k in range(3, Z):
-        g.step(k)
-        if k < Z - 1:
-            g.cross_step(k - 1)
     for s in range(Z):
         landed(c == 1, lat.at[s], dummy.at[2], lrecv.at[s], c)
     for s in range(Z, Z + nk):
@@ -1015,58 +1032,71 @@
         for n in range(Z):
             hsrc[1, n, b * BLOCK : (b + 1) * BLOCK] = both_[n * BLOCK : (n + 1) * BLOCK]
     give(1)
-    if Z > 3:
-        g.cross_step(Z - 2)
-    g.finish()
+    pass_heads(0)
+    out_pass(1)
+    pass_heads(1)
+    for dist in range(2, Z):
+        out_pass(dist)
     for kind in range(2):
-        for k in range(1, Z):
-            zz = lax.rem(z - k + Z, Z)
-            landed(True, hbuf.at[kind, zz], dummy.at[2], hrecv.at[kind, zz], c)
-    hv = jnp.concatenate([hbuf[kind, s] for kind in range(2) for s in range(Z)], axis=1)
-    n = buf.shape[0]
-    half = n // 2
-    rows = hv.shape[0]
-
-    def piece(s, carry):
-        pbuf[s] = dot(hv, buf[s]).astype(BF16)
-        return carry
-
-    lax.fori_loop(0, n, piece, 0)
-    peer = 1 - c
-    copy = pltpu.make_async_remote_copy(
-        src_ref=pbuf.at[pl.ds(peer * half, half)], dst_ref=rbuf, send_sem=tsem.at[0],
-        recv_sem=tsem.at[1], device_id={"tp": peer}, device_id_type=MESH,
-    )
-    copy.start()
-    for p in (W, N, L, H, g):
+        for zz in range(Z):
+            landed(True, hbuf.at[1 - x, kind, zz], dummy.at[2], hrecv.at[1 - x, kind, zz], c)
+    hv = jnp.concatenate(
+        [jnp.concatenate([hbuf[xx, kind, s] for kind in range(2) for s in range(Z)], axis=1)
+         for xx in range(X)], axis=0
+    )
+    rows = hbuf.shape[3]
+    cb = obuf.shape[2]
+    zh = Z // 2
+    for i in range(Z):
+        zz = lax.rem(z + i, Z)
+        if i:
+            landed(True, obuf.at[zz, oyours], dummy.at[0], orecv.at[zz, 1 - y], c)
+        res = dot(hv, obuf[zz]).astype(BF16)
+        owner, at = zz // zh, lax.rem(zz, zh)
+        for xx in range(X):
+            pbuf[zz, xx] = res[xx * rows : (xx + 1) * rows]
+        for to in range(2):
+            R.put(owner == to, pbuf.at[zz, 1 - x], rbuf.at[c, 1, at], precv.at[c, 1, at],
+                  {"fs": 1 - x, "tp": to})
+        R.put(owner != c, pbuf.at[zz, x], rbuf.at[1 - c, 0, at], precv.at[1 - c, 0, at],
+              {"tp": 1 - c})
+    for p in (W, N, L, H, O):
         p.drain()
-    copy.wait()
     total = jnp.zeros((rows, 1), F32)
     mixed = []
-    for s in range(half):
-        m = pbuf[c * half + s].astype(F32) + rbuf[s].astype(F32)
-        mixed.append(m)
+    for at in range(zh):
+        landed(True, rbuf.at[c, 0, at], dummy.at[2], precv.at[c, 0, at], c)
+        m = pbuf[c * zh + at, x].astype(F32) + rbuf[c, 0, at].astype(F32)
+        mixed.append((at * X + x, m))
+        total = total + jnp.sum(m * m, axis=-1, keepdims=True)
+    for at in range(zh):
+        for cc in range(2):
+            landed(True, rbuf.at[cc, 1, at], dummy.at[2], precv.at[cc, 1, at], c)
+        m = rbuf[0, 1, at].astype(F32) + rbuf[1, 1, at].astype(F32)
+        mixed.append((at * X + 1 - x, m))
         total = total + jnp.sum(m * m, axis=-1, keepdims=True)
     sq[0] = jnp.broadcast_to(total, sq.shape[1:])
     squares = pltpu.make_async_remote_copy(
-        src_ref=sq.at[0], dst_ref=sq.at[1], send_sem=tsem.at[2], recv_sem=tsem.at[3],
-        device_id={"tp": peer}, device_id_type=MESH,
+        src_ref=sq.at[0], dst_ref=sq.at[1], send_sem=tsem.at[0], recv_sem=tsem.at[1],
+        device_id={"tp": 1 - c}, device_id_type=MESH,
     )
     squares.start()
+    R.drain()
     squares.wait()
     total = total + sq[1][:, :1]
-    cb = buf.shape[2]
-    norm = lax.rsqrt(total / (n * cb) + NORM_EPS)
-    for s in range(half):
-        out[:, s * cb : (s + 1) * cb] = (mixed[s] * norm * post[s]).astype(BF16)
-
-
-def splits_by_heads(sizes, seqs, count, qw, qd, kd, qup, lup):
+    norm = lax.rsqrt(total / (Z * X * cb) + NORM_EPS)
+    for s, m in mixed:
+        at = pl.ds(pl.multiple_of(s * cb, cb), cb)
+        out[:, at] = (m * norm * post[s]).astype(BF16)
+
+
+def splits_by_heads(sizes, seqs, count, qw, qd, kd, qup, lup, do, lo):
     Y, Z, X, C = sizes
     nk = kd[1] // 128
     return (
         Y == 2 and X == 2 and C == 2 and seqs == C and count == BLOCK and qw[1] == Z * HEAD
-        and qd[1] == Z * 128 and kd[1] == nk * 128 and Z % nk == 0
+        and qd[1] == Z * 128 and kd[1] == nk * 128 and Z % nk == 0 and Z % 2 == 0
+        and do[0] == lo[0]
         and qup[1] == Z * 2 * (NOPE + ROPE) and lup[1] == Z * 2 * (NOPE + VDIM)
     )
 
@@ -1083,14 +1113,14 @@
     nk = latent_down.shape[1] // 128
     cb = delta_out.shape[1]
     depth = delta_out.shape[0] + latent_out.shape[0]
-    cuts = (0, depth * 7 // 16, depth * 14 // 16, depth)
     half = n // 2
     lh = query_up.shape[1] // (NOPE + ROPE) // Z
     total = rows * Z
     ncol = 4 * 128
+    small = [w.T for w in (beta_weight, decay_weight, rope_weight)]
     args = (
         tokens.reshape(rows, width), pre_gain.reshape(1, width),
-        beta_weight, decay_weight, rope_weight,
+        small[0], small[1], small[2],
         query_weight, key_weight, value_weight, query_down, latent_down, delta_out, latent_out,
         query_gain.reshape(1, -1), latent_gain.reshape(1, -1), query_up, latent_up,
         decay_rate.reshape(1, -1), delta_gain.reshape(1, HEAD), post_gain.reshape(half, 1, cb),
@@ -1098,22 +1128,22 @@
     hbm = (0, 2, 3, 4, 5, 6, 7, 8, 9, 10, 11, 14, 15)
     DMA = pltpu.SemaphoreType.DMA
     result = pl.pallas_call(
-        functools.partial(heads_kernel, sizes, seqs, cuts),
+        functools.partial(heads_kernel, sizes, seqs),
         name="layer",
         out_shape=jax.ShapeDtypeStruct((rows, half * cb), BF16),
         in_specs=[anywhere() if i in hbm else vmem() for i in range(len(args))],
         out_specs=vmem(),
         scratch_shapes=[
             pltpu.VMEM((rows, width), BF16),
-            pltpu.VMEM(beta_weight.shape, BF16),
-            pltpu.VMEM(decay_weight.shape, BF16),
-            pltpu.VMEM(rope_weight.shape, BF16),
+            pltpu.VMEM(small[0].shape, BF16),
+            pltpu.VMEM(small[1].shape, BF16),
+            pltpu.VMEM(small[2].shape, BF16),
             pltpu.VMEM(query_up.shape, BF16),
             pltpu.VMEM(latent_up.shape, BF16),
             pltpu.VMEM((Z, shard, ncol), BF16),
             pltpu.VMEM((n, shard, ncol), BF16),
             pltpu.VMEM((seqs, Z, BLOCK, width), BF16),
-            pltpu.VMEM((width, 256), BF16),
+            pltpu.VMEM((256, width), BF16),
             pltpu.VMEM((query_up.shape[0], 2 * lh * 128), BF16),
             pltpu.VMEM((Z * BLOCK, 128), F32),
             pltpu.VMEM((Z * BLOCK, 128), F32),
@@ -1121,11 +1151,10 @@
             pltpu.VMEM((total, 256), F32),
             pltpu.VMEM((Z + nk, total, 128), BF16),
             pltpu.VMEM((2, Z, rows, 128), BF16),
-            pltpu.VMEM((2, Z, rows, 128), BF16),
-            pltpu.VMEM((depth, cb), BF16),
-            pltpu.VMEM((n, depth, cb), BF16),
-            pltpu.VMEM((n, rows, cb), BF16),
-            pltpu.VMEM((half, rows, cb), BF16),
+            pltpu.VMEM((X, 2, Z, rows, 128), BF16),
+            pltpu.VMEM((Z, depth, cb), BF16),
+            pltpu.VMEM((Z, X, rows, cb), BF16),
+            pltpu.VMEM((2, 2, Z // 2, rows, cb), BF16),
             pltpu.VMEM((2, rows, 128), F32),
             DMA((4 * Z + 8,)),
             DMA((4 * Z,)),
@@ -1134,12 +1163,16 @@
             DMA((seqs, Z)),
             DMA((2 * Z + 2 * nk,)),
             DMA((Z + nk,)),
-            DMA((2 * Z,)),
-            DMA((2, Z)),
+            DMA((4 * Z,)),
+            DMA((X, 2, Z)),
+            DMA((4 + 6 * Z,)),
+            DMA((Z, 2)),
+            DMA((3 * Z,)),
+            DMA((2, 2, Z // 2)),
             DMA((1,)),
             DMA((3,)),
-        ]
-        + Gather.scratch(Z, X) + [DMA((6,))],
+            DMA((2,)),
+        ],
         compiler_params=pltpu.CompilerParams(
             collective_id=0, has_side_effects=True, vmem_limit_bytes=60 * 1024 * 1024
         ),

time: 92.4 us -> 88.3 us (0.956); the launches traced: 92.1 us -> 87 us
  local copies, waits for them, and re-layouts: 5.45 us -> 1.67 us
  Pallas kernels: 86.7 us -> 85.3 us
    unnamed x8 -> x1, local copies, waits for them, and re-layouts: 5.45 us -> 1.67 us
    pallas_call x1, Pallas kernels: 86.7 us -> 85.3 us  [by_heads(): pl.pallas_call(functools.partial(heads_kernel, sizes, seqs), name='layer'...]
where the time goes in v2:
time: 88.3 us; the launch traced here: 87 us
  Pallas kernels  85.3 us (97%)
  local copies, waits for them, and re-layouts  1.67 us (2%)
    pallas_call x1, Pallas kernels, by_heads(): pl.pallas_call(functools.partial(heads_kernel, sizes, seqs), name='layer'...  85.3 us

profile of v2, /device:TPU:0, one launch (start us, length us, event | category | flops | bytes accessed | tf_op | source)
XLA Modules:
  0.0 87.0 jit_solution(15987555479426134294)
XLA Ops:
  0.0 85.3 %layer.1 = bf16[128,1024]{1,0:T(8,128)(2,1)} custom-call(bf16[128,2048]{1,0:T(8,128)(2,1)} %bitcast.12, f32[1,2048]{1,0:T(1,128)} %bitcast.16, bf16[8,2048]{1,0:T(8,128)(2,1)} %bitcast.14, bf16[8,2048]{1,0:T(8,128)(2,1)} %bitcast.15, bf16[32,2048]{1,0:T(8,128)(2,1)} %bitcast.13, bf16[256,512]{1,0:T(8,128)(2,1)} %w_query.1, bf16[256,512]{1,0:T(8,128)(2,1)} %w_key.1, ...), custom_call_target="tpu_custom_call" | custom-call | tf_op jit(solution)/shard_map/layer/pallas_call | solution.py:1130
  85.3 1.7 %copy.21 = bf16[2,64,1024]{2,1,0:T(8,128)(2,1)} copy(bf16[2,64,1024]{2,1,0:T(8,128)(2,1)} %bitcast.11) | data formatting | bytes 524288

commit v3 on v2

--- a/solution.py
+++ b/solution.py
@@ -769,10 +769,17 @@
         t = tok[b * BLOCK : (b + 1) * BLOCK].astype(F32)
         scale = lax.rsqrt(jnp.mean(t * t, axis=-1, keepdims=True) + NORM_EPS)
         nbuf[b, z] = (t * scale * pre_gain[...]).astype(BF16)
-    for sign in (1, -1):
-        nxt = z + sign
-        N.put(jnp.logical_and(nxt >= 0, nxt < Z), nbuf.at[c, z], nbuf.at[c, z],
-              nrecv.at[c, z], {"sp": nxt})
+    chunks = nrecv.shape[2]
+    span = BLOCK // chunks
+
+    def chunk(seq, zz, i):
+        return nbuf.at[seq, zz, pl.ds(i * span, span)]
+
+    for i in range(chunks):
+        for sign in (1, -1):
+            nxt = z + sign
+            ref = chunk(c, z, i)
+            N.put(jnp.logical_and(nxt >= 0, nxt < Z), ref, ref, nrecv.at[c, z, i], {"sp": nxt})
 
     for index in rest:
         loads[index]().wait()
@@ -821,9 +828,9 @@
     omine = pl.ds(pl.multiple_of(y * obl, obl), obl)
     oyours = pl.ds(pl.multiple_of((1 - y) * obl, obl), obl)
 
-    def out_send(dist):
+    def out_send():
         for sign in (1, -1):
-            to = z + sign * dist
+            to = z + sign
             ref = obuf.at[z, omine]
             O.put(jnp.logical_and(to >= 0, to < Z), ref, ref, orecv.at[z, y], {"sp": to})
 
@@ -834,9 +841,8 @@
             nxt = z + sign
             ref = obuf.at[zz, omine]
             landed(ok, ref, dummy.at[0], orecv.at[zz, y], c)
-            if dist >= 2:
-                O.put(both(ok, jnp.logical_and(nxt >= 0, nxt < Z)), ref, ref,
-                      orecv.at[zz, y], {"sp": nxt})
+            O.put(both(ok, jnp.logical_and(nxt >= 0, nxt < Z)), ref, ref, orecv.at[zz, y],
+                  {"sp": nxt})
             O.put(ok, ref, ref, orecv.at[zz, y], {"grp": 1 - y})
 
     def wait_w(zz, xx, yy, rows):
@@ -850,17 +856,18 @@
         for dev in ({"fs": 1 - x}, {"grp": 1 - y}, {"fs": 1 - x, "grp": 1 - y}):
             ref = wbuf.at[slot, mine]
             W.put(True, ref, ref, wrecv.at[slot, y], dev)
-        for sign in (1, -1):
-            zz = z - sign * k
-            ok = jnp.logical_and(zz >= 0, zz < Z)
-            nxt = z + sign
-            ref = nbuf.at[c, zz]
-            landed(ok, ref, dummy.at[1], nrecv.at[c, zz], c)
-            N.put(both(ok, jnp.logical_and(nxt >= 0, nxt < Z)), ref, ref, nrecv.at[c, zz],
-                  {"sp": nxt})
-            N.put(ok, ref, ref, nrecv.at[c, zz], {"tp": 1 - c})
+        for i in range(chunks):
+            for sign in (1, -1):
+                zz = z - sign * k
+                ok = jnp.logical_and(zz >= 0, zz < Z)
+                nxt = z + sign
+                ref = chunk(c, zz, i)
+                landed(ok, ref, dummy.at[1], nrecv.at[c, zz, i], c)
+                N.put(both(ok, jnp.logical_and(nxt >= 0, nxt < Z)), ref, ref,
+                      nrecv.at[c, zz, i], {"sp": nxt})
+                N.put(ok, ref, ref, nrecv.at[c, zz, i], {"tp": 1 - c})
         if k == max(1, Z - 2):
-            out_send(1)
+            out_send()
     for k in range(1, Z):
         zz = lax.rem(z - k + Z, Z)
         wait_w(zz, x, 1 - y, yours)
@@ -871,16 +878,14 @@
     keep_own.wait()
     for k in range(1, Z):
         zz = lax.rem(z - k + Z, Z)
-        landed(True, nbuf.at[1 - c, zz], dummy.at[1], nrecv.at[1 - c, zz], c)
+        for i in range(chunks):
+            landed(True, chunk(1 - c, zz, i), dummy.at[1], nrecv.at[1 - c, zz, i], c)
 
     lslot = (1 - c) * z + c * (Z + kblock)
     for b in range(seqs):
         at = slice(b * length, (b + 1) * length)
         normed = nbuf[b].reshape(length, width)
-        pr = dot(normed, wbuf[...].reshape(width, ncol)).astype(BF16)
-        lat[lslot, at] = pr[:, 3 * tile :]
-        raw[at] = pr[:, : 3 * tile]
-        sm[at] = dot_t(normed, ssel[...])
+        lat[lslot, at] = dot(normed, wbuf[:, :, 3 * tile :].reshape(width, tile)).astype(BF16)
 
     def latput(cond, slot, dev):
         L.put(cond, lat.at[slot], lat.at[slot], lrecv.at[slot], dev)
@@ -891,7 +896,11 @@
     for k in range(1, nk):
         latput(c == 1, Z + kblock, {"sp": pair + lax.rem(kblock + k, nk)})
     latput(True, lslot, {"tp": 1 - c})
-    out_send(2)
+    for b in range(seqs):
+        at = slice(b * length, (b + 1) * length)
+        normed = nbuf[b].reshape(length, width)
+        raw[at] = dot(normed, wbuf[:, :, : 3 * tile].reshape(width, 3 * tile)).astype(BF16)
+        sm[at] = dot_t(normed, ssel[...])
 
     ri = lax.broadcasted_iota(jnp.int32, (BLOCK, BLOCK), 0)
     ci = lax.broadcasted_iota(jnp.int32, (BLOCK, BLOCK), 1)
@@ -949,6 +958,7 @@
     inv = [m.astype(BF16) for m in inv]
     nv = [dot(inv[i], terms[i][2].astype(BF16)) for i in every]
     kw = [dot(inv[i], terms[i][3].astype(BF16)).astype(BF16) for i in every]
+    out_pass(1)
     state = [None] * seqs
     for n in range(Z):
         for b in range(seqs):
@@ -1033,9 +1043,9 @@
             hsrc[1, n, b * BLOCK : (b + 1) * BLOCK] = both_[n * BLOCK : (n + 1) * BLOCK]
     give(1)
     pass_heads(0)
-    out_pass(1)
+    out_pass(2)
     pass_heads(1)
-    for dist in range(2, Z):
+    for dist in range(3, Z):
         out_pass(dist)
     for kind in range(2):
         for zz in range(Z):
@@ -1047,8 +1057,9 @@
     rows = hbuf.shape[3]
     cb = obuf.shape[2]
     zh = Z // 2
+    way = 1 - 2 * (z // zh)
     for i in range(Z):
-        zz = lax.rem(z + i, Z)
+        zz = lax.rem(z + way * i + Z, Z)
         if i:
             landed(True, obuf.at[zz, oyours], dummy.at[0], orecv.at[zz, 1 - y], c)
         res = dot(hv, obuf[zz]).astype(BF16)
@@ -1117,6 +1128,7 @@
     lh = query_up.shape[1] // (NOPE + ROPE) // Z
     total = rows * Z
     ncol = 4 * 128
+    chunks = 4
     small = [w.T for w in (beta_weight, decay_weight, rope_weight)]
     args = (
         tokens.reshape(rows, width), pre_gain.reshape(1, width),
@@ -1159,8 +1171,8 @@
             DMA((4 * Z + 8,)),
             DMA((4 * Z,)),
             DMA((n, 2)),
-            DMA((2 + 4 * Z,)),
-            DMA((seqs, Z)),
+            DMA((2 * chunks + 4 * Z * chunks,)),
+            DMA((seqs, Z, chunks)),
             DMA((2 * Z + 2 * nk,)),
             DMA((Z + nk,)),
             DMA((4 * Z,)),

time: 88.3 us -> 75.8 us (0.86); the launches traced: 87 us -> 75.7 us
  Pallas kernels: 85.3 us -> 74 us
    pallas_call x1, Pallas kernels: 85.3 us -> 74 us  [by_heads(): pl.pallas_call(functools.partial(heads_kernel, sizes, seqs), name='layer'...]
where the time goes in v3:
time: 75.8 us; the launch traced here: 75.7 us
  Pallas kernels  74 us (98%)
  local copies, waits for them, and re-layouts  1.67 us (2%)
    pallas_call x1, Pallas kernels, by_heads(): pl.pallas_call(functools.partial(heads_kernel, sizes, seqs), name='layer'...  74 us
    unnamed x1, local copies, waits for them, and re-layouts  1.67 us

profile of v3, /device:TPU:0, one launch (start us, length us, event | category | flops | bytes accessed | tf_op | source)
XLA Modules:
  0.0 75.7 jit_solution(12175318618695375633)
XLA Ops:
  0.0 74.0 %layer.1 = bf16[128,1024]{1,0:T(8,128)(2,1)} custom-call(bf16[128,2048]{1,0:T(8,128)(2,1)} %bitcast.12, f32[1,2048]{1,0:T(1,128)} %bitcast.16, bf16[8,2048]{1,0:T(8,128)(2,1)} %bitcast.14, bf16[8,2048]{1,0:T(8,128)(2,1)} %bitcast.15, bf16[32,2048]{1,0:T(8,128)(2,1)} %bitcast.13, bf16[256,512]{1,0:T(8,128)(2,1)} %w_query.1, bf16[256,512]{1,0:T(8,128)(2,1)} %w_key.1, ...), custom_call_target="tpu_custom_call" | custom-call | tf_op jit(solution)/shard_map/layer/pallas_call | solution.py:1142
  74.0 1.7 %copy.21 = bf16[2,64,1024]{2,1,0:T(8,128)(2,1)} copy(bf16[2,64,1024]{2,1,0:T(8,128)(2,1)} %bitcast.11) | data formatting | bytes 524288

commit v4 on v3

--- a/solution.py
+++ b/solution.py
@@ -656,6 +656,16 @@
     return result.reshape(seqs, count, half * cb)
 
 
+def cut(a):
+    high = a.astype(BF16)
+    return high, (a - high.astype(F32)).astype(BF16)
+
+
+def dot3(a, b, f=dot):
+    (ah, al), (bh, bl) = cut(a), cut(b)
+    return f(ah, bh) + (f(ah, bl) + f(al, bh))
+
+
 class Puts:
     def __init__(self, sems):
         self.sems, self.sent = sems, []
@@ -942,7 +952,7 @@
         gap = gcol - grow
         decay = jnp.where(causal, jnp.exp(jnp.where(causal, gap, 0.0)), 0.0)
         ks = k * beta
-        low = jnp.where(strict, dot_t(ks, k, HIGHEST) * decay, 0.0)
+        low = jnp.where(strict, dot3(ks, k, dot_t) * decay, 0.0)
         scores = dot_t(q.astype(BF16), k.astype(BF16)) * decay
         eg = jnp.exp(gcol)
         terms.append([low, scores, v * beta, ks * eg, q * eg, k * jnp.exp(glast - gcol),
@@ -952,8 +962,8 @@
     size = 2
     while size < BLOCK:
         joint = (ri // (2 * size) == ci // (2 * size)) & (ri // size != ci // size)
-        mids = [dot(jnp.where(joint, terms[i][0], 0.0), inv[i], HIGHEST) for i in every]
-        inv = [inv[i] - dot(inv[i], mids[i], HIGHEST) for i in every]
+        mids = [dot3(jnp.where(joint, terms[i][0], 0.0), inv[i]) for i in every]
+        inv = [inv[i] - dot3(inv[i], mids[i]) for i in every]
         size *= 2
     inv = [m.astype(BF16) for m in inv]
     nv = [dot(inv[i], terms[i][2].astype(BF16)) for i in every]

time: 75.8 us -> 75.5 us (level)
  no operation moved by 1% of the time
where the time goes in v4:
time: 75.5 us; the launch traced here: 75.3 us
  Pallas kernels  73.6 us (97%)
  local copies, waits for them, and re-layouts  1.67 us (2%)
    pallas_call x1, Pallas kernels, by_heads(): pl.pallas_call(functools.partial(heads_kernel, sizes, seqs), name='layer'...  73.6 us
    unnamed x1, local copies, waits for them, and re-layouts  1.67 us

profile of v4, /device:TPU:0, one launch (start us, length us, event | category | flops | bytes accessed | tf_op | source)
XLA Modules:
  0.0 75.3 jit_solution(5156715120311669708)
XLA Ops:
  0.0 73.6 %layer.1 = bf16[128,1024]{1,0:T(8,128)(2,1)} custom-call(bf16[128,2048]{1,0:T(8,128)(2,1)} %bitcast.12, f32[1,2048]{1,0:T(1,128)} %bitcast.16, bf16[8,2048]{1,0:T(8,128)(2,1)} %bitcast.14, bf16[8,2048]{1,0:T(8,128)(2,1)} %bitcast.15, bf16[32,2048]{1,0:T(8,128)(2,1)} %bitcast.13, bf16[256,512]{1,0:T(8,128)(2,1)} %w_query.1, bf16[256,512]{1,0:T(8,128)(2,1)} %w_key.1, ...), custom_call_target="tpu_custom_call" | custom-call | tf_op jit(solution)/shard_map/layer/pallas_call | solution.py:1152
  73.6 1.7 %copy.21 = bf16[2,64,1024]{2,1,0:T(8,128)(2,1)} copy(bf16[2,64,1024]{2,1,0:T(8,128)(2,1)} %bitcast.11) | data formatting | bytes 524288
